TPU v7x, 32 devices: a whole 2x2x4 slice. The times are simulated.
32 devices in a mesh: ep: 4 (over y, x), tp: 8 (over z, core).
Axes of the slice: x: 2, y: 2, z: 4, core: 2. Of those that a mesh axis runs over, the one named last changes fastest.
Arguments:
- tokens: bfloat16 [64, 4096], P('ep'), may hold values from -150 to 150
- query_weight: bfloat16 [4096, 1024], P('tp'), may hold values from -0.09375 to 0.09375
- key_weight: bfloat16 [4096, 1024], P('tp'), may hold values from -0.09375 to 0.09375
- value_weight: bfloat16 [4096, 2048], P(None, 'tp'), may hold values from -0.09375 to 0.09375
- decay_down: bfloat16 [4096, 16], replicated, may hold values from -0.09375 to 0.09375
- decay_up: float32 [16, 1024], replicated, may hold values from -3 to 3
- decay_bias: float32 [1024], replicated, may hold values from -8 to 4
- old_state: float32 [64, 256, 2048], P('ep', None, 'tp'), may hold values from -8 to 8
- out_weight: bfloat16 [2048, 4096], P('tp'), may hold values from -0.1875 to 0.1875
- norm_gain: float32 [4096], replicated, may hold values from 0.2 to 4
- router_weight: bfloat16 [4096, 4], replicated, may hold values from -0.09375 to 0.09375
- routing: int32 [64, 2], P('ep'), may hold values from 0 to 3, all different within a row; in each aligned block of 16 rows (0 to 15, 16 to 31, ...) at most 16 rows name the same one
- glu_weight: bfloat16 [4, 4096, 2048], P('ep', None, 'tp'), may hold values from -0.25 to 0.25
- linear_weight: bfloat16 [4, 4096, 2048], P('ep', None, 'tp'), may hold values from -0.25 to 0.25
- down_weight: bfloat16 [4, 2048, 4096], P('ep', 'tp'), may hold values from -0.01953125 to 0.01953125
- final_gain: float32 [4096], replicated, may hold values from 0.1 to 1.9
Outputs:
- layer_out: bfloat16 [64, 4096], P('ep', 'tp')
- new_state: float32 [64, 256, 2048], P('ep', None, 'tp')
Inputs may be any that keep to these rules, and one draw needn't show every extreme that they name: `routing`: within the rows of one device (aligned blocks of 16 rows) no expert is named by more than 16 rows, and at least one block reaches that bound; each row names 2 different experts.
All inputs are finite; a program needn't handle non-finite values.
Results may differ from a plain program's by a relative error of at most 0.015.
Values may be sent and summed in bfloat16 or wider, within the bound.
A program may use at most 64 MiB of HBM per device.

v0:
```python
import jax
import jax.numpy as jnp
from jax import lax
from jax.sharding import PartitionSpec as P

ALPHA = 2.0**0.25
TAU = 16.0
LIMIT = 7.0
SLOPE = 1.702
EPSILON = 1e-05


def norm_from_totals(inputs, totals, width, gain):
    mean = totals[0][:, None] / width
    variance = totals[1][:, None] / width - mean * mean
    return (inputs - mean) * lax.rsqrt(variance + EPSILON) * gain


def row_totals(inputs):
    return (jnp.sum(inputs, axis=1), jnp.sum(inputs * inputs, axis=1))


def clamped_unit(glu_pre, linear_pre):
    glu = jnp.minimum(glu_pre, LIMIT)
    linear = jnp.clip(linear_pre, -LIMIT, LIMIT)
    return glu * jax.nn.sigmoid(SLOPE * glu) * (linear + 1.0)


def expert_gate(logits, slot_ids, own_expert):
    expert_ids = jnp.arange(logits.shape[1], dtype=jnp.int32)
    picked = jnp.sum(
        jnp.where(slot_ids[:, :, None] == expert_ids[None, None, :], logits[:, None, :], 0.0),
        axis=2,
    )
    own_logit = jnp.sum(jnp.where(expert_ids[None, :] == own_expert, logits, 0.0), axis=1)
    return jnp.exp(own_logit) / jnp.sum(jnp.exp(picked), axis=1)


def per_device(
    tokens,
    query_weight,
    key_weight,
    value_weight,
    decay_down,
    decay_up,
    decay_bias,
    old_state,
    out_weight,
    norm_gain,
    router_weight,
    routing,
    glu_weight,
    linear_weight,
    down_weight,
    final_gain,
):
    tp_count = lax.axis_size("tp")
    tp_rank = lax.axis_index("tp")
    own_expert = lax.axis_index("ep")
    seq_count, width = tokens.shape
    head_dk = old_state.shape[1]
    heads = query_weight.shape[1] // head_dk
    head_start = tp_rank // (tp_count // heads) * head_dk
    top_count = routing.shape[1]
    experts = router_weight.shape[1]
    slot_cap = max(2, (2 * seq_count * top_count + experts - 1) // experts)
    share_width = width // tp_count
    share_start = tp_rank * share_width
    glu_local = glu_weight[0]
    linear_local = linear_weight[0]
    down_local = down_weight[0]
    token_share = lax.dynamic_slice_in_dim(tokens, share_start, share_width, 1)
    query_part = jnp.dot(token_share, query_weight, preferred_element_type=jnp.float32)
    key_part = jnp.dot(token_share, key_weight, preferred_element_type=jnp.float32)
    query_sum, key_sum = lax.psum((query_part, key_part), "tp")
    query_all = query_sum.astype(jnp.bfloat16)
    key_all = key_sum.astype(jnp.bfloat16)
    values = jnp.dot(tokens, value_weight, preferred_element_type=jnp.float32).astype(jnp.bfloat16)
    low_rank = jnp.dot(tokens, decay_down, preferred_element_type=jnp.float32)
    up_cols = lax.dynamic_slice_in_dim(decay_up, head_start, head_dk, 1)
    bias_cols = lax.dynamic_slice_in_dim(decay_bias, head_start, head_dk, 0)
    decay = jnp.exp(
        jax.nn.log_sigmoid(jnp.dot(low_rank, up_cols, precision=lax.Precision.HIGHEST) + bias_cols)
        / TAU
    )
    query = lax.dynamic_slice_in_dim(query_all, head_start, head_dk, 1).astype(jnp.float32)
    keys = lax.dynamic_slice_in_dim(key_all, head_start, head_dk, 1).astype(jnp.float32)
    new_state = (
        decay[:, :, None] * old_state + keys[:, :, None] * values.astype(jnp.float32)[:, None, :]
    )
    mixed = (
        jnp.einsum("si,sic->sc", query, new_state, precision=lax.Precision.HIGHEST)
        * head_dk ** (-0.5)
    ).astype(jnp.bfloat16)
    out_terms = jnp.dot(mixed, out_weight, preferred_element_type=jnp.float32)
    flat_ids = routing.reshape(-1)
    expert_ids = jnp.arange(experts, dtype=jnp.int32)
    chosen = (flat_ids[:, None] == expert_ids[None, :]).astype(jnp.int32)
    before = jnp.cumsum(chosen, axis=0) - chosen
    slot_rank = jnp.sum(before * chosen, axis=1)
    slot_index = flat_ids * slot_cap + slot_rank
    placed = (
        slot_index[:, None] == jnp.arange(experts * slot_cap, dtype=jnp.int32)[None, :]
    ).astype(jnp.int32)
    spread = jnp.sum(placed.reshape(seq_count, top_count, experts * slot_cap), axis=1)
    spread_rows = spread.astype(jnp.bfloat16)
    slot_ids = jnp.einsum("sn,sk->nk", spread, routing).reshape(experts, slot_cap, top_count)
    projected = lax.psum_scatter(out_terms, "tp", scatter_dimension=1, tiled=True)
    hidden_in = ALPHA * token_share.astype(jnp.float32) + projected
    first = lax.psum(row_totals(hidden_in), "tp")
    gain_share = lax.dynamic_slice_in_dim(norm_gain, share_start, share_width, 0)
    normed = norm_from_totals(hidden_in, first, width, gain_share).astype(jnp.bfloat16)
    send_rows = jnp.einsum(
        "sn,sd->nd", spread_rows, normed, preferred_element_type=jnp.float32
    ).astype(jnp.bfloat16)
    send_rows = send_rows.reshape(experts, slot_cap, normed.shape[1])
    rows_in = lax.all_to_all(send_rows, "ep", split_axis=0, concat_axis=0, tiled=True)
    ids_in = lax.all_to_all(slot_ids, "ep", split_axis=0, concat_axis=0, tiled=True)
    sources, slots, row_width = rows_in.shape
    count = sources * slots
    piece = lax.all_gather(rows_in, "tp", axis=2, tiled=True)
    size = piece.shape[2]
    flat = piece.reshape(count, size)
    glu_pre = jnp.dot(flat, glu_local, preferred_element_type=jnp.float32)
    linear_pre = jnp.dot(flat, linear_local, preferred_element_type=jnp.float32)
    logits = jnp.dot(flat, router_weight, preferred_element_type=jnp.float32)
    act = clamped_unit(glu_pre, linear_pre).astype(jnp.bfloat16)
    summed = lax.psum_scatter(
        jnp.dot(act, down_local, preferred_element_type=jnp.float32),
        "tp",
        scatter_dimension=1,
        tiled=True,
    )
    gate = expert_gate(logits, ids_in.reshape(count, top_count), own_expert)
    weighted = (
        (summed * gate[:, None]).astype(jnp.bfloat16).reshape(sources, slots, summed.shape[1])
    )
    returned = lax.all_to_all(weighted, "ep", split_axis=0, concat_axis=0, tiled=True)
    combined = ALPHA * normed.astype(jnp.float32) + jnp.einsum(
        "sn,nd->sd",
        spread_rows,
        returned.reshape(experts * slot_cap, normed.shape[1]),
        preferred_element_type=jnp.float32,
    )
    second = lax.psum(row_totals(combined), "tp")
    final_share = lax.dynamic_slice_in_dim(final_gain, share_start, share_width, 0)
    layer_out = norm_from_totals(combined, second, width, final_share).astype(jnp.bfloat16)
    return (layer_out, new_state)


def solution(mesh):
    return jax.shard_map(
        per_device,
        mesh=mesh,
        in_specs=(
            P("ep", None),
            P("tp", None),
            P("tp", None),
            P(None, "tp"),
            P(),
            P(),
            P(),
            P("ep", None, "tp"),
            P("tp", None),
            P(),
            P(),
            P("ep", None),
            P("ep", None, "tp"),
            P("ep", None, "tp"),
            P("ep", "tp", None),
            P(),
        ),
        out_specs=(P("ep", "tp"), P("ep", None, "tp")),
        check_vma=False,
    )
```

profile of v0, /device:TPU:0, one launch (start us, length us, event | category | flops | bytes accessed | tf_op | source)
XLA Modules:
  0.0 188.1 jit_solution(6148383914185210825)
XLA Ops:
  7.3 1.6 fusion.43
  8.9 1.5 fusion.45
  10.4 31.6 %all-reduce.4 = (bf16[16,1024]{1,0:T(8,128)(2,1)S(1)}, bf16[16,1024]{1,0:T(8,128)(2,1)S(1)}) all-reduce(f32[16,1024]{1,0:T(8,128)S(1)} %fusion.43, f32[16,1024]{1,0:T(8,128)S(1)} %fusion.45), channel_id=1, replica_groups=mesh['ep'=4,'tp'=8] {'tp'}, use_global_device_ids=true, to_apply=%region_1.2 | all-reduce | flops 32768 | bytes 196608 | tf_op jit(solution)/shard_map/psum | solution.py:75
  42.9 2.0 %fusion.24 = f32[16,256]{1,0:T(8,128)S(1)} fusion(bf16[16,4096]{1,0:T(8,128)(2,1)S(1)} %copy-done.3, bf16[4096,256]{1,0:T(8,128)(2,1)} %param.19), kind=kOutput, calls=%fused_computation.17 | convolution fusion | flops 33562624 | bytes 2244608 | tf_op jit(solution)/shard_map/dot_general | solution.py:78
  44.9 0.9 fusion.37
  45.8 2.9 %multiply_add_fusion = f32[16,256,256]{2,1,0:T(8,128)S(1)} fusion(f32[16,256,256]{2,1,0:T(8,128)} %param.23, f32[16,256]{1,0:T(8,128)S(1)} %fusion.24, f32[16,256]{1,0:T(8,128)S(1)} %fusion.50, f32[16,256]{1,0:T(8,128)S(1)} %fusion.37), kind=kLoop, calls=%fused_computation | loop fusion | flops 3145728 | bytes 8437760 | tf_op jit(solution)/shard_map/add | solution.py:89
  48.7 1.5 fusion.39
  50.8 1.0 copy-done.2
  51.8 1.1 fusion.47
  54.5 27.6 %reduce-scatter.3.cloned.1.call-done = f32[16,512]{1,0:T(8,128)} async-done(((f32[16,4096]{1,0:T(8,128)}), f32[16,512]{1,0:T(8,128)}) %reduce-scatter.3.cloned.1.call-update) | async-done | bytes 32784 | tf_op jit(solution)/shard_map/reduce_scatter | solution.py:108
  82.1 0.9 fusion.52
  83.0 13.7 %all-reduce.1 = (f32[16]{0:T(128)S(1)}, f32[16]{0:T(128)S(1)}) all-reduce(f32[16]{0:T(128)S(1)} %get-tuple-element.3, f32[16]{0:T(128)S(1)} %get-tuple-element.2), channel_id=1, replica_groups=mesh['ep'=4,'tp'=8] {'tp'}, use_global_device_ids=true, to_apply=%region_6.7 | all-reduce | flops 32 | bytes 256 | tf_op jit(solution)/shard_map/psum | solution.py:110
  97.7 8.5 %all_to_all.15 = bf16[4,16,512]{2,1,0:T(8,128)(2,1)S(1)} all-to-all(bf16[4,16,512]{2,1,0:T(8,128)(2,1)S(1)} %bitcast.58), channel_id=1, replica_groups=mesh['ep'=4,'tp'=8] {'ep'}, dimensions={0} | all-to-all | bytes 131072 | tf_op jit(solution)/shard_map/all_to_all | solution.py:117
  106.3 14.9 %all_gather.3 = bf16[4,16,4096]{2,1,0:T(8,128)(2,1)S(1)} all-gather(bf16[4,16,512]{2,1,0:T(8,128)(2,1)S(1)} %all_to_all.15), channel_id=1, replica_groups=mesh['ep'=4,'tp'=8] {'tp'}, dimensions={2}, use_global_device_ids=true | all-gather | bytes 589824 | tf_op jit(solution)/shard_map/all_gather | solution.py:121
  121.2 2.0 %fusion.6 = f32[64,256]{1,0:T(8,128)S(1)} fusion(bf16[64,4096]{1,0:T(8,128)(2,1)S(1)} %bitcast.55, bf16[1,4096,256]{2,1,0:T(8,128)(2,1)} %param.28), kind=kOutput, calls=%fused_computation.8 | convolution fusion | flops 134234112 | bytes 2686976 | tf_op jit(solution)/shard_map/dot_general | solution.py:124
  123.3 4.0 %fusion = f32[64,4096]{1,0:T(8,128)} fusion(bf16[1,256,4096]{2,1,0:T(8,128)(2,1)S(1)} %copy-done, bf16[64,4096]{1,0:T(8,128)(2,1)S(1)} %bitcast.56, bf16[1,4096,256]{2,1,0:T(8,128)(2,1)} %param.29, f32[64,256]{1,0:T(8,128)S(1)} %fusion.6), kind=kOutput, calls=%fused_computation.1 | convolution fusion | flops 268582912 | bytes 5832704 | tf_op jit(solution)/shard_map/dot_general | solution.py:129
  127.4 1.1 fusion.55
  128.5 3.2 %all-to-all-start.1 = ((s32[4,16,2]{1,2,0:T(2,128)}), s32[4,16,2]{1,2,0:T(2,128)S(1)}, u32[]{:S(2)}, u32[]{:S(2)}) async-start(s32[4,16,2]{1,2,0:T(2,128)} %fusion.55), calls=%async_computation.3 | async-start | bytes 8192 | tf_op jit(solution)/shard_map/all_to_all | solution.py:118
  131.7 4.6 %all-to-all-done.1 = s32[4,16,2]{1,2,0:T(2,128)S(1)} async-done(((s32[4,16,2]{1,2,0:T(2,128)}), s32[4,16,2]{1,2,0:T(2,128)S(1)}, u32[]{:S(2)}, u32[]{:S(2)}) %all-to-all-start.1) | async-done | bytes 544 | tf_op jit(solution)/shard_map/all_to_all | solution.py:118
  136.8 19.8 %reduce-scatter.5.cloned.1.call-done = f32[64,512]{1,0:T(8,128)} async-done(((f32[64,4096]{1,0:T(8,128)}), f32[64,512]{1,0:T(8,128)}) %reduce-scatter.5.cloned.1.call-update) | async-done | bytes 131088 | tf_op jit(solution)/shard_map/reduce_scatter | solution.py:128
  156.6 1.6 multiply_convert_fusion
  158.2 3.7 %all-to-all-start.2 = ((bf16[4,16,512]{2,1,0:T(8,128)(2,1)}), bf16[4,16,512]{2,1,0:T(8,128)(2,1)S(1)}, u32[]{:S(2)}, u32[]{:S(2)}) async-start(bf16[4,16,512]{2,1,0:T(8,128)(2,1)} %bitcast.10), calls=%async_computation.4 | async-start | bytes 131072 | tf_op jit(solution)/shard_map/all_to_all | solution.py:138
  162.7 4.1 %all-to-all-done.2 = bf16[4,16,512]{2,1,0:T(8,128)(2,1)S(1)} async-done(((bf16[4,16,512]{2,1,0:T(8,128)(2,1)}), bf16[4,16,512]{2,1,0:T(8,128)(2,1)S(1)}, u32[]{:S(2)}, u32[]{:S(2)}) %all-to-all-start.2) | async-done | bytes 65568 | tf_op jit(solution)/shard_map/all_to_all | solution.py:138
  167.0 13.6 %all-reduce = (f32[16]{0:T(128)S(1)}, f32[16]{0:T(128)S(1)}) all-reduce(f32[16]{0:T(128)S(1)} %get-tuple-element.5, f32[16]{0:T(128)S(1)} %get-tuple-element.4), channel_id=1, replica_groups=mesh['ep'=4,'tp'=8] {'tp'}, use_global_device_ids=true, to_apply=%region_17.18 | all-reduce | flops 32 | bytes 256 | tf_op jit(solution)/shard_map/psum | solution.py:145
  (46 shorter events, 6.4 us)
Async XLA Ops:
  7.2 116.1 %copy-start = (bf16[1,256,4096]{2,1,0:T(8,128)(2,1)S(1)}, bf16[1,256,4096]{2,1,0:T(8,128)(2,1)}, u32[]{:S(2)}) copy-start(bf16[1,256,4096]{2,1,0:T(8,128)(2,1)} %param.30) | copy-start | bytes 6291460
  7.2 35.6 %copy-start.3 = (bf16[16,4096]{1,0:T(8,128)(2,1)S(1)}, bf16[16,4096]{1,0:T(8,128)(2,1)}, u32[]{:S(2)}) copy-start(bf16[16,4096]{1,0:T(8,128)(2,1)} %param.16) | copy-start | bytes 393220
  7.2 35.6 %copy-start.4 = (bf16[4096,16]{0,1:T(8,128)(2,1)S(1)}, bf16[4096,16]{0,1:T(8,128)(2,1)}, u32[]{:S(2)}) copy-start(bf16[4096,16]{0,1:T(8,128)(2,1)} %param.20) | copy-start | bytes 393220
  7.2 74.9 %reduce-scatter.3.cloned.1.call-start = ((), (), s32[]{:S(2)}) async-start(), calls=%async_computation.5 | async-start | bytes 294912 | tf_op jit(solution)/shard_map/reduce_scatter | solution.py:108
  48.7 2.1 %copy-start.1 = (f32[16,256,256]{2,1,0:T(8,128)}, f32[16,256,256]{2,1,0:T(8,128)S(1)}, u32[]{:S(2)}) copy-start(f32[16,256,256]{2,1,0:T(8,128)S(1)} %multiply_add_fusion) | copy-start | bytes 12582916
  48.7 3.1 %copy-start.2 = (bf16[256,4096]{1,0:T(8,128)(2,1)S(1)}, bf16[256,4096]{1,0:T(8,128)(2,1)}, u32[]{:S(2)}) copy-start(bf16[256,4096]{1,0:T(8,128)(2,1)} %param.24) | copy-start | bytes 6291460
  51.8 1.2 copy-start.5
  52.9 103.7 %reduce-scatter.5.cloned.1.call-start = ((), (), s32[]{:S(2)}) async-start(), calls=%async_computation.6 | async-start | bytes 1179648 | tf_op jit(solution)/shard_map/reduce_scatter | solution.py:128
  123.3 13.2 %copy-start.6 = (bf16[4096,4]{0,1:T(4,128)(2,1)S(1)}, bf16[4096,4]{0,1:T(4,128)(2,1)}, u32[]{:S(2)}) copy-start(bf16[4096,4]{0,1:T(4,128)(2,1)} %param.26) | copy-start | bytes 98308
  128.5 7.9 %all-to-all-start.1 = ((s32[4,16,2]{1,2,0:T(2,128)}), s32[4,16,2]{1,2,0:T(2,128)S(1)}, u32[]{:S(2)}, u32[]{:S(2)}) async-start(s32[4,16,2]{1,2,0:T(2,128)} %fusion.55), calls=%async_computation.3 | async-start | bytes 8192 | tf_op jit(solution)/shard_map/all_to_all | solution.py:118
  158.2 8.6 %all-to-all-start.2 = ((bf16[4,16,512]{2,1,0:T(8,128)(2,1)}), bf16[4,16,512]{2,1,0:T(8,128)(2,1)S(1)}, u32[]{:S(2)}, u32[]{:S(2)}) async-start(bf16[4,16,512]{2,1,0:T(8,128)(2,1)} %bitcast.10), calls=%async_computation.4 | async-start | bytes 131072 | tf_op jit(solution)/shard_map/all_to_all | solution.py:138
Sparse Core Ops, SparseCore 0:
  53.0 28.9 reduce-scatter.2
  127.4 29.1 reduce-scatter.4
where the time goes:
time: 189 us; the launch traced here: 188 us
  blocking collectives  82.4 us (44%)
  waiting for transfers between devices  56.2 us (30%)
  matrix products  16.6 us (9%)
  between operations  14.2 us (8%)
  other arithmetic  7.34 us (4%)
  starting transfers between devices  7.03 us (4%)
  local copies, waits for them, and re-layouts  4.41 us (2%)
    psum x1, blocking collectives, per_device(): query_sum, key_sum = lax.psum((query_part, key_part), 'tp')  31.6 us
    reduce_scatter x1, waiting for transfers between devices, per_device(): lax.psum_scatter(out_terms, 'tp', scatter_dimension=1, tiled=True)  27.6 us
    reduce_scatter x1, waiting for transfers between devices, per_device(): lax.psum_scatter(jnp.dot(act, down_local, preferred_element_type=jnp.floa...  19.8 us
    all_gather x1, blocking collectives, per_device(): piece = lax.all_gather(rows_in, 'tp', axis=2, tiled=True)  14.9 us
    psum x1, blocking collectives, per_device(): first = lax.psum(row_totals(hidden_in), 'tp')  13.7 us
    psum x1, blocking collectives, per_device(): second = lax.psum(row_totals(combined), 'tp')  13.6 us
    all_to_all x1, blocking collectives, per_device(): lax.all_to_all(send_rows, 'ep', split_axis=0, concat_axis=0, tiled=True)  8.53 us
    all_to_all x1, waiting for transfers between devices, per_device(): lax.all_to_all(slot_ids, 'ep', split_axis=0, concat_axis=0, tiled=True)  4.63 us
  transfers between devices with their start and end apart: 4, of which 4 were waited for; matrix products, arithmetic and copies ran while one was open for 2% of the time, Pallas kernels for 0%

commit v1 on v0

--- a/solution.py
+++ b/solution.py
@@ -118,7 +118,21 @@
     ids_in = lax.all_to_all(slot_ids, "ep", split_axis=0, concat_axis=0, tiled=True)
     sources, slots, row_width = rows_in.shape
     count = sources * slots
-    piece = lax.all_gather(rows_in, "tp", axis=2, tiled=True)
+    ways, here, step = (lax.axis_size("tp"), lax.axis_index("tp"), rows_in.shape[2])
+    dims = [n * ways if d == 2 else n for d, n in enumerate(rows_in.shape)]
+    full = lax.dynamic_update_slice_in_dim(
+        jnp.zeros(dims, rows_in.dtype), rows_in, here * step, axis=2
+    )
+    going_up = going_down = rows_in
+    for far in range(1, ways // 2 + 1):
+        going_up = lax.ppermute(going_up, "tp", [(d, (d + 1) % ways) for d in range(ways)])
+        full = lax.dynamic_update_slice_in_dim(full, going_up, (here - far) % ways * step, axis=2)
+        if 2 * far < ways:
+            going_down = lax.ppermute(going_down, "tp", [(d, (d - 1) % ways) for d in range(ways)])
+            full = lax.dynamic_update_slice_in_dim(
+                full, going_down, (here + far) % ways * step, axis=2
+            )
+    piece = full
     size = piece.shape[2]
     flat = piece.reshape(count, size)
     glu_pre = jnp.dot(flat, glu_local, preferred_element_type=jnp.float32)

time: 189 us -> 197 us (1.042)
  blocking collectives: 82.4 us -> 58.9 us
  waiting for transfers between devices: 56.2 us -> 72.3 us
  starting transfers between devices: 7.03 us -> 21.6 us
    all_gather x1 -> x0, blocking collectives: 14.9 us -> none  [per_device(): piece = lax.all_gather(rows_in, 'tp', axis=2, tiled=True)]
    ppermute x0 -> x7, waiting for transfers between devices: none -> 11.3 us  [the longest x4 11.3 us: per_device(): lax.ppermute(going_up, 'tp', [(d, (d + 1) % ways) for d in range(ways)])]
    ppermute x0 -> x7, starting transfers between devices: none -> 10.6 us  [the longest x3 10.6 us: per_device(): lax.ppermute(going_down, 'tp', [(d, (d - 1) % ways) for d in range(ways)])]
    all_to_all x1 -> x0, blocking collectives: 8.53 us -> none  [per_device(): lax.all_to_all(send_rows, 'ep', split_axis=0, concat_axis=0, tiled=True)]
    all_to_all x0 -> x1, waiting for transfers between devices: none -> 4.84 us  [per_device(): lax.all_to_all(send_rows, 'ep', split_axis=0, concat_axis=0, tiled=True)]
    all_to_all x0 -> x1, starting transfers between devices: none -> 3.88 us  [per_device(): lax.all_to_all(send_rows, 'ep', split_axis=0, concat_axis=0, tiled=True)]
  transfers between devices with their start and end apart: 4 -> 12, of which waited for: 4 -> 9; matrix products, arithmetic and copies ran while one was open for 2% -> 2% of each run, Pallas kernels for 0% -> 0%
where the time goes in v1:
time: 197 us; the launch traced here: 196 us
  waiting for transfers between devices  72.3 us (37%)
  blocking collectives  58.9 us (30%)
  starting transfers between devices  21.6 us (11%)
  matrix products  17.2 us (9%)
  between operations  14.3 us (7%)
  other arithmetic  7.34 us (4%)
  local copies, waits for them, and re-layouts  4.53 us (2%)
    psum x1, blocking collectives, per_device(): query_sum, key_sum = lax.psum((query_part, key_part), 'tp')  31.6 us
    reduce_scatter x1, waiting for transfers between devices, per_device(): lax.psum_scatter(out_terms, 'tp', scatter_dimension=1, tiled=True)  27.7 us
    reduce_scatter x1, waiting for transfers between devices, per_device(): lax.psum_scatter(jnp.dot(act, down_local, preferred_element_type=jnp.floa...  19.8 us
    psum x1, blocking collectives, per_device(): first = lax.psum(row_totals(hidden_in), 'tp')  13.7 us
    psum x1, blocking collectives, per_device(): second = lax.psum(row_totals(combined), 'tp')  13.6 us
    ppermute x4, waiting for transfers between devices, per_device(): lax.ppermute(going_up, 'tp', [(d, (d + 1) % ways) for d in range(ways)])  11.3 us
    ppermute x3, starting transfers between devices, per_device(): lax.ppermute(going_down, 'tp', [(d, (d - 1) % ways) for d in range(ways)])  10.6 us
    all_to_all x1, waiting for transfers between devices, per_device(): lax.all_to_all(send_rows, 'ep', split_axis=0, concat_axis=0, tiled=True)  4.84 us
  transfers between devices with their start and end apart: 12, of which 9 were waited for; matrix products, arithmetic and copies ran while one was open for 2% of the time, Pallas kernels for 0%

profile of v1, /device:TPU:0, one launch (start us, length us, event | category | flops | bytes accessed | tf_op | source)
XLA Modules:
  0.0 196.2 jit_solution(13733827087048339835)
XLA Ops:
  7.3 1.6 fusion.33
  10.4 31.6 %all-reduce.4 = (bf16[16,1024]{1,0:T(8,128)(2,1)S(1)}, bf16[16,1024]{1,0:T(8,128)(2,1)S(1)}) all-reduce(f32[16,1024]{1,0:T(8,128)S(1)} %fusion.33, f32[16,1024]{1,0:T(8,128)S(1)} %fusion.35), channel_id=1, replica_groups=mesh['ep'=4,'tp'=8] {'tp'}, use_global_device_ids=true, to_apply=%region_1.2 | all-reduce | flops 32768 | bytes 196608 | tf_op jit(solution)/shard_map/psum | solution.py:75
  42.9 2.0 %fusion.16 = f32[16,256]{1,0:T(8,128)S(1)} fusion(bf16[16,4096]{1,0:T(8,128)(2,1)S(1)} %copy-done.3, bf16[4096,256]{1,0:T(8,128)(2,1)} %param.19), kind=kOutput, calls=%fused_computation.15 | convolution fusion | flops 33562624 | bytes 2244608 | tf_op jit(solution)/shard_map/dot_general | solution.py:78
  45.8 2.9 %multiply_add_fusion = f32[16,256,256]{2,1,0:T(8,128)S(1)} fusion(f32[16,256,256]{2,1,0:T(8,128)} %param.23, f32[16,256]{1,0:T(8,128)S(1)} %fusion.16, f32[16,256]{1,0:T(8,128)S(1)} %fusion.40, f32[16,256]{1,0:T(8,128)S(1)} %fusion.27), kind=kLoop, calls=%fused_computation | loop fusion | flops 3145728 | bytes 8437760 | tf_op jit(solution)/shard_map/add | solution.py:89
  54.4 27.7 %reduce-scatter.3.cloned.1.call-done = f32[16,512]{1,0:T(8,128)} async-done(((f32[16,4096]{1,0:T(8,128)}), f32[16,512]{1,0:T(8,128)}) %reduce-scatter.3.cloned.1.call-update) | async-done | bytes 32784 | tf_op jit(solution)/shard_map/reduce_scatter | solution.py:108
  83.0 13.7 %all-reduce.1 = (f32[16]{0:T(128)S(1)}, f32[16]{0:T(128)S(1)}) all-reduce(f32[16]{0:T(128)S(1)} %get-tuple-element.3, f32[16]{0:T(128)S(1)} %get-tuple-element.2), channel_id=1, replica_groups=mesh['ep'=4,'tp'=8] {'tp'}, use_global_device_ids=true, to_apply=%region_6.7 | all-reduce | flops 32 | bytes 256 | tf_op jit(solution)/shard_map/psum | solution.py:110
  98.4 3.9 %all-to-all-start = ((bf16[4,16,512]{2,1,0:T(8,128)(2,1)}), bf16[4,16,512]{2,1,0:T(8,128)(2,1)S(1)}, u32[]{:S(2)}, u32[]{:S(2)}) async-start(bf16[4,16,512]{2,1,0:T(8,128)(2,1)} %bitcast.2), calls=%async_computation.1 | async-start | bytes 131072 | tf_op jit(solution)/shard_map/all_to_all | solution.py:117
  102.3 4.8 %all-to-all-done = bf16[4,16,512]{2,1,0:T(8,128)(2,1)S(1)} async-done(((bf16[4,16,512]{2,1,0:T(8,128)(2,1)}), bf16[4,16,512]{2,1,0:T(8,128)(2,1)S(1)}, u32[]{:S(2)}, u32[]{:S(2)}) %all-to-all-start) | async-done | bytes 65568 | tf_op jit(solution)/shard_map/all_to_all | solution.py:117
  107.1 3.5 %collective-permute-start.1 = (bf16[4,16,512]{2,1,0:T(8,128)(2,1)S(1)}, bf16[4,16,512]{2,1,0:T(8,128)(2,1)S(1)}, u32[]{:S(2)}, u32[]{:S(2)}) collective-permute-start(bf16[4,16,512]{2,1,0:T(8,128)(2,1)S(1)} %all-to-all-done), channel_id=1, source_target_pairs={{0,7},{1,0},{2,1},{3,2},{4,3},{5,4},{6,5},{7,6},{8,15},{9,8},{10,9... | collective-permute-start | bytes 196616 | tf_op jit(solution)/shard_map/ppermute | solution.py:131
  110.7 1.9 collective-permute-done
  112.6 3.5 %collective-permute-start.3 = (bf16[4,16,512]{2,1,0:T(8,128)(2,1)S(1)}, bf16[4,16,512]{2,1,0:T(8,128)(2,1)S(1)}, u32[]{:S(2)}, u32[]{:S(2)}) collective-permute-start(bf16[4,16,512]{2,1,0:T(8,128)(2,1)S(1)} %collective-permute-done.1), channel_id=1, source_target_pairs={{0,7},{1,0},{2,1},{3,2},{4,3},{5,4},{6,5},{7,6},{8,15},{9,8},{10,9... | collective-permute-start | bytes 196616 | tf_op jit(solution)/shard_map/ppermute | solution.py:131
  116.2 2.0 %collective-permute-done.2 = bf16[4,16,512]{2,1,0:T(8,128)(2,1)S(1)} collective-permute-done((bf16[4,16,512]{2,1,0:T(8,128)(2,1)S(1)}, bf16[4,16,512]{2,1,0:T(8,128)(2,1)S(1)}, u32[]{:S(2)}, u32[]{:S(2)}) %collective-permute-start.2) | collective-permute-done | bytes 65568 | tf_op jit(solution)/shard_map/ppermute | solution.py:128
  118.2 3.5 %collective-permute-start.5 = (bf16[4,16,512]{2,1,0:T(8,128)(2,1)S(1)}, bf16[4,16,512]{2,1,0:T(8,128)(2,1)S(1)}, u32[]{:S(2)}, u32[]{:S(2)}) collective-permute-start(bf16[4,16,512]{2,1,0:T(8,128)(2,1)S(1)} %collective-permute-done.3), channel_id=1, source_target_pairs={{0,7},{1,0},{2,1},{3,2},{4,3},{5,4},{6,5},{7,6},{8,15},{9,8},{10,9... | collective-permute-start | bytes 196616 | tf_op jit(solution)/shard_map/ppermute | solution.py:131
  121.8 1.9 collective-permute-done.4
  123.8 5.4 %collective-permute-done.6 = bf16[4,16,512]{2,1,0:T(8,128)(2,1)S(1)} collective-permute-done((bf16[4,16,512]{2,1,0:T(8,128)(2,1)S(1)}, bf16[4,16,512]{2,1,0:T(8,128)(2,1)S(1)}, u32[]{:S(2)}, u32[]{:S(2)}) %collective-permute-start.6) | collective-permute-done | bytes 65568 | tf_op jit(solution)/shard_map/ppermute | solution.py:128
  129.2 2.1 %fusion.6 = f32[64,256]{1,0:T(8,128)S(1)} fusion(bf16[64,4096]{1,0:T(8,128)(2,1)S(1)} %bitcast.53, bf16[1,4096,256]{2,1,0:T(8,128)(2,1)} %param.28), kind=kOutput, calls=%fused_computation.8 | convolution fusion | flops 134234112 | bytes 2686976 | tf_op jit(solution)/shard_map/dot_general | solution.py:138
  131.3 4.0 %fusion = f32[64,4096]{1,0:T(8,128)} fusion(bf16[1,256,4096]{2,1,0:T(8,128)(2,1)S(1)} %copy-done, f32[64,256]{1,0:T(8,128)S(1)} %fusion.6, bf16[64,4096]{1,0:T(8,128)(2,1)S(1)} %bitcast.54, bf16[1,4096,256]{2,1,0:T(8,128)(2,1)} %param.29), kind=kOutput, calls=%fused_computation.1 | convolution fusion | flops 268582912 | bytes 5832704 | tf_op jit(solution)/shard_map/dot_general | solution.py:143
  136.5 3.2 %all-to-all-start.1 = ((s32[4,16,2]{1,2,0:T(2,128)}), s32[4,16,2]{1,2,0:T(2,128)S(1)}, u32[]{:S(2)}, u32[]{:S(2)}) async-start(s32[4,16,2]{1,2,0:T(2,128)} %fusion.48), calls=%async_computation.3 | async-start | bytes 8192 | tf_op jit(solution)/shard_map/all_to_all | solution.py:118
  139.8 4.6 %all-to-all-done.1 = s32[4,16,2]{1,2,0:T(2,128)S(1)} async-done(((s32[4,16,2]{1,2,0:T(2,128)}), s32[4,16,2]{1,2,0:T(2,128)S(1)}, u32[]{:S(2)}, u32[]{:S(2)}) %all-to-all-start.1) | async-done | bytes 544 | tf_op jit(solution)/shard_map/all_to_all | solution.py:118
  144.8 19.8 %reduce-scatter.5.cloned.1.call-done = f32[64,512]{1,0:T(8,128)} async-done(((f32[64,4096]{1,0:T(8,128)}), f32[64,512]{1,0:T(8,128)}) %reduce-scatter.5.cloned.1.call-update) | async-done | bytes 131088 | tf_op jit(solution)/shard_map/reduce_scatter | solution.py:142
  164.6 1.6 multiply_convert_fusion
  166.2 3.8 %all-to-all-start.2 = ((bf16[4,16,512]{2,1,0:T(8,128)(2,1)}), bf16[4,16,512]{2,1,0:T(8,128)(2,1)S(1)}, u32[]{:S(2)}, u32[]{:S(2)}) async-start(bf16[4,16,512]{2,1,0:T(8,128)(2,1)} %bitcast.10), calls=%async_computation.4 | async-start | bytes 131072 | tf_op jit(solution)/shard_map/all_to_all | solution.py:152
  170.7 4.1 %all-to-all-done.2 = bf16[4,16,512]{2,1,0:T(8,128)(2,1)S(1)} async-done(((bf16[4,16,512]{2,1,0:T(8,128)(2,1)}), bf16[4,16,512]{2,1,0:T(8,128)(2,1)S(1)}, u32[]{:S(2)}, u32[]{:S(2)}) %all-to-all-start.2) | async-done | bytes 65568 | tf_op jit(solution)/shard_map/all_to_all | solution.py:152
  175.0 13.6 %all-reduce = (f32[16]{0:T(128)S(1)}, f32[16]{0:T(128)S(1)}) all-reduce(f32[16]{0:T(128)S(1)} %get-tuple-element.5, f32[16]{0:T(128)S(1)} %get-tuple-element.4), channel_id=1, replica_groups=mesh['ep'=4,'tp'=8] {'tp'}, use_global_device_ids=true, to_apply=%region_17.18 | all-reduce | flops 32 | bytes 256 | tf_op jit(solution)/shard_map/psum | solution.py:159
  (69 shorter events, 15.0 us)
Async XLA Ops:
  7.2 124.1 %copy-start = (bf16[1,256,4096]{2,1,0:T(8,128)(2,1)S(1)}, bf16[1,256,4096]{2,1,0:T(8,128)(2,1)}, u32[]{:S(2)}) copy-start(bf16[1,256,4096]{2,1,0:T(8,128)(2,1)} %param.30) | copy-start | bytes 6291460
  7.2 35.6 %copy-start.3 = (bf16[16,4096]{1,0:T(8,128)(2,1)S(1)}, bf16[16,4096]{1,0:T(8,128)(2,1)}, u32[]{:S(2)}) copy-start(bf16[16,4096]{1,0:T(8,128)(2,1)} %param.16) | copy-start | bytes 393220
  7.2 35.6 %copy-start.4 = (bf16[4096,16]{0,1:T(8,128)(2,1)S(1)}, bf16[4096,16]{0,1:T(8,128)(2,1)}, u32[]{:S(2)}) copy-start(bf16[4096,16]{0,1:T(8,128)(2,1)} %param.20) | copy-start | bytes 393220
  7.2 74.9 %reduce-scatter.3.cloned.1.call-start = ((), (), s32[]{:S(2)}) async-start(), calls=%async_computation.5 | async-start | bytes 294912 | tf_op jit(solution)/shard_map/reduce_scatter | solution.py:108
  48.7 2.1 %copy-start.1 = (f32[16,256,256]{2,1,0:T(8,128)}, f32[16,256,256]{2,1,0:T(8,128)S(1)}, u32[]{:S(2)}) copy-start(f32[16,256,256]{2,1,0:T(8,128)S(1)} %multiply_add_fusion) | copy-start | bytes 12582916
  48.7 3.1 %copy-start.2 = (bf16[256,4096]{1,0:T(8,128)(2,1)S(1)}, bf16[256,4096]{1,0:T(8,128)(2,1)}, u32[]{:S(2)}) copy-start(bf16[256,4096]{1,0:T(8,128)(2,1)} %param.24) | copy-start | bytes 6291460
  51.8 1.1 copy-start.5
  98.4 8.7 %all-to-all-start = ((bf16[4,16,512]{2,1,0:T(8,128)(2,1)}), bf16[4,16,512]{2,1,0:T(8,128)(2,1)S(1)}, u32[]{:S(2)}, u32[]{:S(2)}) async-start(bf16[4,16,512]{2,1,0:T(8,128)(2,1)} %bitcast.2), calls=%async_computation.1 | async-start | bytes 131072 | tf_op jit(solution)/shard_map/all_to_all | solution.py:117
  102.2 62.3 %reduce-scatter.5.cloned.1.call-start = ((), (), s32[]{:S(2)}) async-start(), calls=%async_computation.6 | async-start | bytes 1179648 | tf_op jit(solution)/shard_map/reduce_scatter | solution.py:142
  107.1 5.5 %collective-permute-start = (bf16[4,16,512]{2,1,0:T(8,128)(2,1)S(1)}, bf16[4,16,512]{2,1,0:T(8,128)(2,1)S(1)}, u32[]{:S(2)}, u32[]{:S(2)}) collective-permute-start(bf16[4,16,512]{2,1,0:T(8,128)(2,1)S(1)} %all-to-all-done), channel_id=1, source_target_pairs={{0,1},{1,2},{2,3},{3,4},{4,5},{5,6},{6,7},{7,0},{8,9},{9,10},{10,1... | collective-permute-start | bytes 196616 | tf_op jit(solution)/shard_map/ppermute | solution.py:128
  107.1 5.5 %collective-permute-start.1 = (bf16[4,16,512]{2,1,0:T(8,128)(2,1)S(1)}, bf16[4,16,512]{2,1,0:T(8,128)(2,1)S(1)}, u32[]{:S(2)}, u32[]{:S(2)}) collective-permute-start(bf16[4,16,512]{2,1,0:T(8,128)(2,1)S(1)} %all-to-all-done), channel_id=1, source_target_pairs={{0,7},{1,0},{2,1},{3,2},{4,3},{5,4},{6,5},{7,6},{8,15},{9,8},{10,9... | collective-permute-start | bytes 196616 | tf_op jit(solution)/shard_map/ppermute | solution.py:131
  112.6 5.6 %collective-permute-start.2 = (bf16[4,16,512]{2,1,0:T(8,128)(2,1)S(1)}, bf16[4,16,512]{2,1,0:T(8,128)(2,1)S(1)}, u32[]{:S(2)}, u32[]{:S(2)}) collective-permute-start(bf16[4,16,512]{2,1,0:T(8,128)(2,1)S(1)} %collective-permute-done), channel_id=1, source_target_pairs={{0,1},{1,2},{2,3},{3,4},{4,5},{5,6},{6,7},{7,0},{8,9},{9,10},{10,1... | collective-permute-start | bytes 196616 | tf_op jit(solution)/shard_map/ppermute | solution.py:128
  112.6 5.6 %collective-permute-start.3 = (bf16[4,16,512]{2,1,0:T(8,128)(2,1)S(1)}, bf16[4,16,512]{2,1,0:T(8,128)(2,1)S(1)}, u32[]{:S(2)}, u32[]{:S(2)}) collective-permute-start(bf16[4,16,512]{2,1,0:T(8,128)(2,1)S(1)} %collective-permute-done.1), channel_id=1, source_target_pairs={{0,7},{1,0},{2,1},{3,2},{4,3},{5,4},{6,5},{7,6},{8,15},{9,8},{10,9... | collective-permute-start | bytes 196616 | tf_op jit(solution)/shard_map/ppermute | solution.py:131
  118.2 5.5 %collective-permute-start.4 = (bf16[4,16,512]{2,1,0:T(8,128)(2,1)S(1)}, bf16[4,16,512]{2,1,0:T(8,128)(2,1)S(1)}, u32[]{:S(2)}, u32[]{:S(2)}) collective-permute-start(bf16[4,16,512]{2,1,0:T(8,128)(2,1)S(1)} %collective-permute-done.2), channel_id=1, source_target_pairs={{0,1},{1,2},{2,3},{3,4},{4,5},{5,6},{6,7},{7,0},{8,9},{9,10},{10,1... | collective-permute-start | bytes 196616 | tf_op jit(solution)/shard_map/ppermute | solution.py:128
  118.2 5.5 %collective-permute-start.5 = (bf16[4,16,512]{2,1,0:T(8,128)(2,1)S(1)}, bf16[4,16,512]{2,1,0:T(8,128)(2,1)S(1)}, u32[]{:S(2)}, u32[]{:S(2)}) collective-permute-start(bf16[4,16,512]{2,1,0:T(8,128)(2,1)S(1)} %collective-permute-done.3), channel_id=1, source_target_pairs={{0,7},{1,0},{2,1},{3,2},{4,3},{5,4},{6,5},{7,6},{8,15},{9,8},{10,9... | collective-permute-start | bytes 196616 | tf_op jit(solution)/shard_map/ppermute | solution.py:131
  123.7 5.5 %collective-permute-start.6 = (bf16[4,16,512]{2,1,0:T(8,128)(2,1)S(1)}, bf16[4,16,512]{2,1,0:T(8,128)(2,1)S(1)}, u32[]{:S(2)}, u32[]{:S(2)}) collective-permute-start(bf16[4,16,512]{2,1,0:T(8,128)(2,1)S(1)} %collective-permute-done.4), channel_id=1, source_target_pairs={{0,1},{1,2},{2,3},{3,4},{4,5},{5,6},{6,7},{7,0},{8,9},{9,10},{10,1... | collective-permute-start | bytes 196616 | tf_op jit(solution)/shard_map/ppermute | solution.py:128
  131.3 13.2 %copy-start.6 = (bf16[4096,4]{0,1:T(4,128)(2,1)S(1)}, bf16[4096,4]{0,1:T(4,128)(2,1)}, u32[]{:S(2)}) copy-start(bf16[4096,4]{0,1:T(4,128)(2,1)} %param.26) | copy-start | bytes 98308
  136.5 7.9 %all-to-all-start.1 = ((s32[4,16,2]{1,2,0:T(2,128)}), s32[4,16,2]{1,2,0:T(2,128)S(1)}, u32[]{:S(2)}, u32[]{:S(2)}) async-start(s32[4,16,2]{1,2,0:T(2,128)} %fusion.48), calls=%async_computation.3 | async-start | bytes 8192 | tf_op jit(solution)/shard_map/all_to_all | solution.py:118
  166.2 8.6 %all-to-all-start.2 = ((bf16[4,16,512]{2,1,0:T(8,128)(2,1)}), bf16[4,16,512]{2,1,0:T(8,128)(2,1)S(1)}, u32[]{:S(2)}, u32[]{:S(2)}) async-start(bf16[4,16,512]{2,1,0:T(8,128)(2,1)} %bitcast.10), calls=%async_computation.4 | async-start | bytes 131072 | tf_op jit(solution)/shard_map/all_to_all | solution.py:152
Sparse Core Ops, SparseCore 0:
  53.0 28.9 reduce-scatter.2
  135.4 29.0 reduce-scatter.4
